TPU v7x, 32 devices: a whole 2x2x4 slice. The times are simulated.
32 devices in a mesh: rep: 2 (over y), fs: 4 (over z), tp: 4 (over x, core).
Axes of the slice: x: 2, y: 2, z: 4, core: 2. Of those that a mesh axis runs over, the one named last changes fastest.
Arguments:
- tokens: bfloat16 [2048, 2048], P(('rep', 'fs')), may hold values from -6 to 6
- norm_gains: float32 [3, 2048], replicated, may hold values from 0.1 to 1.9
- gate_weight: float32 [2048, 3072], P('fs', 'tp'), may hold values from -0.125 to 0.125
- up_weight: float32 [2048, 3072], P('fs', 'tp'), may hold values from -0.125 to 0.125
- hidden_scales: float32 [2, 3072], P(None, 'tp'), may hold values from 0.5 to 2
- down_weight: float32 [3072, 2048], P('tp', 'fs'), may hold values from -0.21875 to 0.21875
- down_scale: float32 [2048], P('fs'), may hold values from 0.5 to 2
- mix_in: float32 [2048, 512], P('fs'), may hold values from -0.125 to 0.125
- in_scale: float32 [512], replicated, may hold values from 0.5 to 2
- pool_map: float32 [4, 128, 128], replicated, may hold values from -0.5 to 0.5
- pool_scale: float32 [512], P('tp'), may hold values from 0.5 to 2
- mix_out: float32 [512, 2048], P('tp', 'fs'), may hold values from -0.25 to 0.25
- out_scale: float32 [2048], P('fs'), may hold values from 0.5 to 2
Outputs:
- layer_out: bfloat16 [2048, 2048], P(('rep', 'fs'))
All inputs are finite; a program needn't handle non-finite values.
Results may differ from a plain program's by a relative error of at most 0.02.
Values may be sent and summed in bfloat16 or wider, within the bound.
A program may use at most 64 MiB of HBM per device.

v0:
```python
import jax
import jax.numpy as jnp
from jax import lax
from jax.sharding import PartitionSpec as P

eps = 1e-06
widest = 16


def normed(values, gain):
    mean_sq = jnp.mean(values * values, axis=-1, keepdims=True)
    return (values * lax.rsqrt(mean_sq + eps) * gain).astype(jnp.bfloat16)


def scatter_rows(term_fn, share):
    return lax.psum_scatter(
        term_fn(jnp.int32(0), lax.axis_size("tp") * share).astype(jnp.bfloat16),
        "tp",
        scatter_dimension=0,
        tiled=True,
    ).astype(jnp.float32)


def whole_rows(values):
    return lax.all_gather(values, "tp", axis=0, tiled=True)


def fetch_mixer(in_cols, mix_out):
    return (
        lax.all_gather(in_cols.astype(jnp.bfloat16), "fs", axis=0, tiled=True),
        lax.all_gather(mix_out.astype(jnp.bfloat16), "fs", axis=1, tiled=True),
    )


def hidden_units(rows_in, gate_full, up_full, hidden_scales):
    gate = jnp.dot(rows_in, gate_full, preferred_element_type=jnp.float32) * hidden_scales[0]
    upper = jnp.dot(rows_in, up_full, preferred_element_type=jnp.float32) * hidden_scales[1]
    return (jax.nn.silu(gate) * upper).astype(jnp.bfloat16)


def ffn_partial(normed_rows, gate_full, up_full, down_full, hidden_scales, share):

    def term_rows(row_start, row_count):
        hidden = hidden_units(normed_rows, gate_full, up_full, hidden_scales)
        return jnp.dot(hidden, down_full, preferred_element_type=jnp.float32)

    return scatter_rows(term_rows, share)


def per_device(
    tokens,
    norm_gains,
    gate_weight,
    up_weight,
    hidden_scales,
    down_weight,
    down_scale,
    mix_in,
    in_scale,
    pool_map,
    pool_scale,
    mix_out,
    out_scale,
):
    tp_width = lax.axis_size("tp")
    tp_rank = lax.axis_index("tp")
    seq_rows = tokens.shape[0]
    share = seq_rows // tp_width
    local_channels = mix_out.shape[0]
    group_width = pool_map.shape[1]
    needed = max(group_width, local_channels)
    first_channel = tp_rank * local_channels
    in_start = first_channel // group_width * group_width
    in_cols = lax.dynamic_slice_in_dim(mix_in, in_start, needed, 1)
    scale_cols = lax.dynamic_slice_in_dim(in_scale, in_start, needed, 0)
    down_cols, out_cols = (
        lax.all_gather(down_scale, "fs", axis=0, tiled=True),
        lax.all_gather(out_scale, "fs", axis=0, tiled=True),
    )
    gate_bf = gate_weight.astype(jnp.bfloat16)
    up_bf = up_weight.astype(jnp.bfloat16)
    down_bf = down_weight.astype(jnp.bfloat16)
    resid_all = tokens.astype(jnp.float32)
    first = normed(resid_all, norm_gains[0])
    gate_full, up_full, down_full = (
        lax.all_gather(gate_bf, "fs", axis=0, tiled=True),
        lax.all_gather(up_bf, "fs", axis=0, tiled=True),
        lax.all_gather(down_bf, "fs", axis=1, tiled=True),
    )
    ffn_one = ffn_partial(first, gate_full, up_full, down_full, hidden_scales, share)
    own_rows = lax.dynamic_slice_in_dim(resid_all, tp_rank * share, share, 0)
    resid_one = own_rows + 0.5 * (ffn_one * down_cols)
    second = whole_rows(normed(resid_one, norm_gains[1]))
    in_full, out_full = fetch_mixer(in_cols, mix_out)
    pool_in = (jnp.dot(second, in_full, preferred_element_type=jnp.float32) * scale_cols).astype(
        jnp.bfloat16
    )
    channel = in_start + jnp.arange(needed, dtype=jnp.int32)
    window = jnp.left_shift(jnp.int32(2), channel // group_width)
    position = jnp.arange(seq_rows, dtype=jnp.int32)[:, None]
    values = pool_in.astype(jnp.float32)
    summed = jnp.zeros_like(values)
    for offset in range(widest):
        shifted = jnp.pad(values, ((offset, 0), (0, 0)))[:seq_rows]
        summed = summed + jnp.where(offset < window, shifted, 0.0)
    counts = jnp.minimum(position + 1, window).astype(jnp.float32)
    pooled = (summed / counts - values).astype(jnp.bfloat16)
    map_bf = pool_map.astype(jnp.bfloat16)
    if local_channels < group_width:
        group_index = first_channel // group_width
        column_start = first_channel % group_width
        map_cols = lax.dynamic_slice(
            map_bf, (group_index, jnp.int32(0), column_start), (1, group_width, local_channels)
        )[0]
        grouped = jnp.dot(pooled, map_cols, preferred_element_type=jnp.float32)
    else:
        held_groups = local_channels // group_width
        maps_held = lax.dynamic_slice_in_dim(map_bf, first_channel // group_width, held_groups, 0)
        grouped = jnp.einsum(
            "tgc,gcd->tgd",
            pooled.reshape(seq_rows, held_groups, group_width),
            maps_held,
            preferred_element_type=jnp.float32,
        ).reshape(seq_rows, local_channels)
    pool_out = (grouped * pool_scale).astype(jnp.bfloat16)

    def mixer_rows(row_start, row_count):
        return jnp.dot(pool_out, out_full, preferred_element_type=jnp.float32)

    mixed = scatter_rows(mixer_rows, share)
    resid_two = resid_one + mixed * out_cols
    third = whole_rows(normed(resid_two, norm_gains[2]))
    ffn_two = ffn_partial(third, gate_full, up_full, down_full, hidden_scales, share)
    final_rows = (resid_two + 0.5 * (ffn_two * down_cols)).astype(jnp.bfloat16)
    return whole_rows(final_rows)


def solution(mesh):
    return jax.shard_map(
        per_device,
        mesh=mesh,
        in_specs=(
            P(("rep", "fs"), None),
            P(),
            P("fs", "tp"),
            P("fs", "tp"),
            P(None, "tp"),
            P("tp", "fs"),
            P("fs"),
            P("fs", None),
            P(),
            P(),
            P("tp"),
            P("tp", "fs"),
            P("fs"),
        ),
        out_specs=P(("rep", "fs"), None),
        check_vma=False,
    )
```

profile of v0, /device:TPU:0, one launch (start us, length us, event | category | flops | bytes accessed | tf_op | source)
XLA Modules:
  0.0 379.5 jit_solution(11079390840828098439)
XLA Ops:
  6.5 0.0 copy-start
  6.5 0.0 all-gather.9.cloned.1.call-start
  6.5 2.4 convert_element_type.104
  9.0 0.0 all-gather.9.cloned.1.call-update
  9.0 0.0 copy-start.5
  9.0 0.0 copy-start.1
  9.0 0.0 copy-start.4
  9.0 0.0 all-gather.13.cloned.1.call-start
  9.1 2.5 convert_element_type.107
  11.6 0.0 all-gather.13.cloned.1.call-update
  11.6 0.0 all-gather.11.cloned.1.call-start
  11.6 2.4 convert_element_type.105
  14.0 0.0 all-gather.11.cloned.1.call-update
  14.0 0.0 reduce-scatter.4.cloned.1.call-start
  14.1 0.0 copy-done.5
  14.1 0.0 copy-done.1
  14.1 0.3 multiply_reduce_fusion
  14.4 0.0 copy-done.4
  14.5 60.9 %all-gather.9.cloned.1.call-done = bf16[2048,768]{1,0:T(8,128)(2,1)} async-done(((bf16[512,768]{1,0:T(8,128)(2,1)}), bf16[2048,768]{1,0:T(8,128)(2,1)}) %all-gather.9.cloned.1.call-update) | async-done | bytes 3145744 | tf_op jit(solution)/shard_map/all_gather | solution.py:86
  75.3 3.8 convolution_multiply_fusion.3
  79.1 59.9 %all-gather.13.cloned.1.call-done = bf16[768,2048]{1,0:T(8,128)(2,1)} async-done(((bf16[768,512]{1,0:T(8,128)(2,1)}), bf16[768,2048]{1,0:T(8,128)(2,1)}) %all-gather.13.cloned.1.call-update) | async-done | bytes 3145744 | tf_op jit(solution)/shard_map/all_gather | solution.py:88
  139.0 63.7 %all-gather.11.cloned.1.call-done = bf16[2048,768]{1,0:T(8,128)(2,1)} async-done(((bf16[512,768]{1,0:T(8,128)(2,1)}), bf16[2048,768]{1,0:T(8,128)(2,1)}) %all-gather.11.cloned.1.call-update) | async-done | bytes 3145744 | tf_op jit(solution)/shard_map/all_gather | solution.py:87
  202.7 6.2 %convolution_convert_fusion.2 = bf16[256,2048]{1,0:T(8,128)(2,1)} fusion(bf16[768,2048]{1,0:T(8,128)(2,1)} %all-gather.13.cloned.1.call-done, bf16[2048,768]{1,0:T(8,128)(2,1)} %all-gather.11.cloned.1.call-done, f32[256,768]{1,0:T(8,128)} %convolution_multiply_fusion.3, f32[768]{0:T(1024)S(1)} %get-tuple-element.5, f32[2048]{0:T(1024)S(1)} %bitcast.42, ...), kind=kOutput, calls=%fused_computation.2 | convolution fusion | flops 1614610432 | bytes 9187328 | tf_op jit(solution)/shard_map/dot_general | solution.py:45
  209.0 0.0 copy-start.6
  209.0 0.0 copy-start.3
  209.0 0.0 reduce-scatter.4.cloned.1.call-update
  209.0 0.0 all-gather.15.cloned.1.call-start
  209.0 1.5 convert_element_type.102
  210.6 0.0 copy-done.6
  210.6 12.1 %all-gather = f32[4,1,512]{2,1,0:T(1,128)S(1)} all-gather(f32[1,1,512]{2,1,0:T(1,128)S(1)} %bitcast.43), channel_id=1, replica_groups=mesh['rep'=2,'fs'=4,'tp'=4] {'fs'}, dimensions={0}, use_global_device_ids=true | all-gather | bytes 10240 | tf_op jit(solution)/shard_map/all_gather | solution.py:77
  222.7 10.0 %reduce-scatter.4.cloned.1.call-done = bf16[64,2048]{1,0:T(8,128)(2,1)} async-done(((bf16[256,2048]{1,0:T(8,128)(2,1)}), bf16[64,2048]{1,0:T(8,128)(2,1)}) %reduce-scatter.4.cloned.1.call-update) | async-done | bytes 262160 | tf_op jit(solution)/shard_map/reduce_scatter | solution.py:16
  232.6 1.3 multiply_reduce_fusion.2
  234.0 0.8 multiply_convert_fusion.2
  234.8 0.0 all-gather.15.cloned.1.call-update
  234.8 0.0 reduce-scatter.6.cloned.1.call-start
  234.9 0.0 copy-done.3
  234.9 0.8 dynamic_slice.15
  235.9 0.0 copy-done
  235.9 15.4 %all_gather.36 = bf16[128,2048]{1,0:T(8,128)(2,1)S(1)} all-gather(bf16[128,512]{1,0:T(8,128)(2,1)S(1)} %convert_element_type.118), channel_id=1, replica_groups=mesh['rep'=2,'fs'=4,'tp'=4] {'fs'}, dimensions={1}, use_global_device_ids=true | all-gather | bytes 655360 | tf_op jit(solution)/shard_map/all_gather | solution.py:31
  251.4 16.2 %all_gather.35 = bf16[2048,128]{1,0:T(8,128)(2,1)S(1)} all-gather(bf16[512,128]{1,0:T(8,128)(2,1)S(1)} %dynamic-slice_convert_fusion), channel_id=1, replica_groups=mesh['rep'=2,'fs'=4,'tp'=4] {'fs'}, dimensions={0}, use_global_device_ids=true | all-gather | bytes 655360 | tf_op jit(solution)/shard_map/all_gather | solution.py:30
  267.5 1.7 fusion.6
  269.2 0.0 copy-done.8
  269.2 2.7 convolution_convert_fusion
  272.0 0.0 reduce-scatter.6.cloned.1.call-update
  272.0 0.0 all-gather.17.cloned.1.call-start
  272.0 0.0 copy-done.7
  272.0 12.2 %all-gather.1 = f32[4,1,512]{2,1,0:T(1,128)S(1)} all-gather(f32[1,1,512]{2,1,0:T(1,128)S(1)} %bitcast.44), channel_id=1, replica_groups=mesh['rep'=2,'fs'=4,'tp'=4] {'fs'}, dimensions={0}, use_global_device_ids=true | all-gather | bytes 10240 | tf_op jit(solution)/shard_map/all_gather | solution.py:78
  284.3 13.4 %reduce-scatter.6.cloned.1.call-done = bf16[64,2048]{1,0:T(8,128)(2,1)} async-done(((bf16[256,2048]{1,0:T(8,128)(2,1)}), bf16[64,2048]{1,0:T(8,128)(2,1)}) %reduce-scatter.6.cloned.1.call-update) | async-done | bytes 262160 | tf_op jit(solution)/shard_map/reduce_scatter | solution.py:16
  297.7 1.1 multiply_reduce_fusion.1
  298.9 1.8 multiply_convert_fusion.1
  300.6 0.0 all-gather.17.cloned.1.call-update
  300.7 0.0 reduce-scatter.8.cloned.1.call-start
  300.7 16.8 %all-gather.17.cloned.1.call-done = bf16[256,2048]{1,0:T(8,128)(2,1)} async-done(((bf16[64,2048]{1,0:T(8,128)(2,1)}), bf16[256,2048]{1,0:T(8,128)(2,1)}) %all-gather.17.cloned.1.call-update) | async-done | bytes 1048592 | tf_op jit(solution)/shard_map/all_gather | solution.py:25
  317.5 3.2 convolution_multiply_fusion.1
  320.7 0.0 copy-start.2
  320.7 6.3 %convolution_convert_fusion.1 = bf16[256,2048]{1,0:T(8,128)(2,1)} fusion(bf16[768,2048]{1,0:T(8,128)(2,1)} %all-gather.13.cloned.1.call-done, bf16[256,2048]{1,0:T(8,128)(2,1)} %all-gather.17.cloned.1.call-done, bf16[2048,768]{1,0:T(8,128)(2,1)} %all-gather.11.cloned.1.call-done, f32[256,768]{1,0:T(8,128)S(1)} %convolution_multiply_fusion.1, ...), kind=kOutput, calls=%fused_computation.1 | convolution fusion | flops 1612513280 | bytes 9178112 | tf_op jit(solution)/shard_map/dot_general | solution.py:45
  327.0 0.0 reduce-scatter.8.cloned.1.call-update
  327.1 0.0 all-gather.19.cloned.1.call-start
  327.1 24.9 %reduce-scatter.8.cloned.1.call-done = bf16[64,2048]{1,0:T(8,128)(2,1)} async-done(((bf16[256,2048]{1,0:T(8,128)(2,1)}), bf16[64,2048]{1,0:T(8,128)(2,1)}) %reduce-scatter.8.cloned.1.call-update) | async-done | bytes 262160 | tf_op jit(solution)/shard_map/reduce_scatter | solution.py:16
  352.0 0.0 copy-done.2
  352.0 1.8 add_convert_fusion
  353.8 0.0 all-gather.19.cloned.1.call-update
  353.8 16.9 %all-gather.19.cloned.1.call-done = bf16[256,2048]{1,0:T(8,128)(2,1)} async-done(((bf16[64,2048]{1,0:T(8,128)(2,1)}), bf16[256,2048]{1,0:T(8,128)(2,1)}) %all-gather.19.cloned.1.call-update) | async-done | bytes 1048592 | tf_op jit(solution)/shard_map/all_gather | solution.py:25
  370.6 2.3 copy.15
  (20 shorter events, 0.3 us)
Async XLA Ops:
  6.5 229.3 %copy-start = (f32[512,512]{1,0:T(8,128)S(1)}, f32[512,512]{1,0:T(8,128)}, u32[]{:S(2)}) copy-start(f32[512,512]{1,0:T(8,128)} %param.20) | copy-start | bytes 3145732
  6.5 68.8 %all-gather.9.cloned.1.call-start = ((), (), s32[]{:S(2)}) async-start(), calls=%async_computation.3 | async-start | bytes 3932160 | tf_op jit(solution)/shard_map/all_gather | solution.py:86
  9.0 5.1 %copy-start.5 = (f32[2,768]{1,0:T(2,128)S(1)}, f32[2,768]{1,0:T(2,128)}, u32[]{:S(2)}) copy-start(f32[2,768]{1,0:T(2,128)} %param.17) | copy-start | bytes 18436
  9.0 5.1 %copy-start.1 = (bf16[256,2048]{1,0:T(8,128)(2,1)S(1)}, bf16[256,2048]{1,0:T(8,128)(2,1)}, u32[]{:S(2)}) copy-start(bf16[256,2048]{1,0:T(8,128)(2,1)} %param.13) | copy-start | bytes 3145732
  9.0 5.4 %copy-start.4 = (f32[3,2048]{1,0:T(4,128)S(1)}, f32[3,2048]{1,0:T(4,128)}, u32[]{:S(2)}) copy-start(f32[3,2048]{1,0:T(4,128)} %param.14) | copy-start | bytes 73732
  9.0 130.0 %all-gather.13.cloned.1.call-start = ((), (), s32[]{:S(2)}) async-start(), calls=%async_computation.5 | async-start | bytes 3932160 | tf_op jit(solution)/shard_map/all_gather | solution.py:88
  11.6 191.1 %all-gather.11.cloned.1.call-start = ((), (), s32[]{:S(2)}) async-start(), calls=%async_computation.4 | async-start | bytes 3932160 | tf_op jit(solution)/shard_map/all_gather | solution.py:87
  14.0 218.6 %reduce-scatter.4.cloned.1.call-start = ((), (), s32[]{:S(2)}) async-start(), calls=%async_computation.6 | async-start | bytes 1310720 | tf_op jit(solution)/shard_map/reduce_scatter | solution.py:16
  209.0 1.6 copy-start.6
  209.0 25.9 %copy-start.3 = (f32[128,512]{1,0:T(8,128)S(1)}, f32[128,512]{1,0:T(8,128)}, u32[]{:S(2)}) copy-start(f32[128,512]{1,0:T(8,128)} %param.24) | copy-start | bytes 786436
  209.0 58.5 %all-gather.15.cloned.1.call-start = ((), (), s32[]{:S(2)}) async-start(), calls=%async_computation.7 | async-start | bytes 1310720 | tf_op jit(solution)/shard_map/all_gather | solution.py:25
  210.6 58.6 %copy-start.8 = (f32[128]{0:T(128)S(1)}, f32[128]{0:T(128)}, u32[]{:S(2)}) copy-start(f32[128]{0:T(128)} %param.23) | copy-start | bytes 1540
  234.8 62.9 %reduce-scatter.6.cloned.1.call-start = ((), (), s32[]{:S(2)}) async-start(), calls=%async_computation.8 | async-start | bytes 1310720 | tf_op jit(solution)/shard_map/reduce_scatter | solution.py:16
  267.5 4.5 %copy-start.7 = (f32[512]{0:T(512)S(1)}, f32[512]{0:T(512)}, u32[]{:S(2)}) copy-start(f32[512]{0:T(512)} %param.25) | copy-start | bytes 6148
  272.0 45.5 %all-gather.17.cloned.1.call-start = ((), (), s32[]{:S(2)}) async-start(), calls=%async_computation.9 | async-start | bytes 1310720 | tf_op jit(solution)/shard_map/all_gather | solution.py:25
  300.7 51.3 %reduce-scatter.8.cloned.1.call-start = ((), (), s32[]{:S(2)}) async-start(), calls=%async_computation.10 | async-start | bytes 1310720 | tf_op jit(solution)/shard_map/reduce_scatter | solution.py:16
  320.7 31.3 %copy-start.2 = (bf16[64,2048]{1,0:T(8,128)(2,1)S(1)}, bf16[64,2048]{1,0:T(8,128)(2,1)}, u32[]{:S(2)}) copy-start(bf16[64,2048]{1,0:T(8,128)(2,1)} %reduce-scatter.6.cloned.1.call-done) | copy-start | bytes 786436
  327.1 43.6 %all-gather.19.cloned.1.call-start = ((), (), s32[]{:S(2)}) async-start(), calls=%async_computation.11 | async-start | bytes 1310720 | tf_op jit(solution)/shard_map/all_gather | solution.py:25
Sparse Core Ops, SparseCore 0:
  9.1 66.1 all-gather.8
  76.9 62.0 all-gather.12
  140.6 62.0 all-gather.10
  209.1 23.4 reduce-scatter.3
  234.9 16.7 all-gather.14
  272.1 25.5 reduce-scatter.5
  300.8 16.6 all-gather.16
  327.2 24.7 reduce-scatter.7
  353.9 16.6 all-gather.18
where the time goes:
time: 380 us; the launch traced here: 379 us
  waiting for transfers between devices  267 us (70%)
  blocking collectives  55.9 us (15%)
  matrix products  23.9 us (6%)
  other arithmetic  16.1 us (4%)
  between operations  13.4 us (4%)
    all_gather x1, waiting for transfers between devices, per_device(): lax.all_gather(up_bf, 'fs', axis=0, tiled=True)  63.7 us
    all_gather x1, waiting for transfers between devices, per_device(): lax.all_gather(gate_bf, 'fs', axis=0, tiled=True)  60.9 us
    all_gather x1, waiting for transfers between devices, per_device(): lax.all_gather(down_bf, 'fs', axis=1, tiled=True)  59.9 us
    reduce_scatter x3, waiting for transfers between devices, scatter_rows(): lax.psum_scatter(term_fn(jnp.int32(0), lax.axis_size('tp') * share).astyp...  48.3 us
    all_gather x3, waiting for transfers between devices, whole_rows(): return lax.all_gather(values, 'tp', axis=0, tiled=True)  33.7 us
    all_gather x1, blocking collectives, fetch_mixer(): lax.all_gather(in_cols.astype(jnp.bfloat16), 'fs', axis=0, tiled=True)  16.2 us
    all_gather x1, blocking collectives, fetch_mixer(): lax.all_gather(mix_out.astype(jnp.bfloat16), 'fs', axis=1, tiled=True)  15.4 us
    dot_general x2, matrix products, term_rows(): return jnp.dot(hidden, down_full, preferred_element_type=jnp.float32)  12.6 us
  transfers between devices with their start and end apart: 9, of which 8 were waited for; matrix products, arithmetic and copies ran while one was open for 3% of the time, Pallas kernels for 0%

commit v1 on v0

--- a/solution.py
+++ b/solution.py
@@ -1,6 +1,10 @@
+import functools
+
 import jax
 import jax.numpy as jnp
 from jax import lax
+from jax.experimental import pallas as pl
+from jax.experimental.pallas import tpu as pltpu
 from jax.sharding import PartitionSpec as P
 
 eps = 1e-06
@@ -135,9 +139,423 @@
     return whole_rows(final_rows)
 
 
+MESH = pl.DeviceIdType.MESH
+QUARTERS = 4
+TILE = 256
+bf16 = jnp.bfloat16
+f32 = jnp.float32
+
+
+def fits_kernel(mesh):
+    return mesh.shape["rep"] == 2 and mesh.shape["fs"] == 4 and mesh.shape["tp"] == 4
+
+
+def layer_kernel(
+    n, tok, gains, gu_in, hs, dn_in, wi_in, wo_in, isc, pmap, ps_in, sc_in,
+    out, gu_buf, dn_buf, wi_all, wo_all, sc_all, ps_all,
+    first, gacc, hidden, stage, rs, r1, second, pool, r2, third, rs_a, s_b, rs_b,
+    ring_send, ring_recv, sc_send, sc_recv, tp_send, tp_recv, rs_send, rs_recv, ag_send, ag_recv, loc,
+):
+    rep, fs, me = lax.axis_index("rep"), lax.axis_index("fs"), lax.axis_index("tp")
+    width = tok.shape[1]
+    seq = tok.shape[0]
+    slab = width // n
+    share = seq // 4
+    halo = widest
+    units = hs.shape[1]
+    gc = pmap.shape[1]
+    core = me % 2
+    mate = me + 1 - 2 * core
+    across = (me + 2) % 4
+    diag = (mate + 2) % 4
+    peers = {1: mate, 2: across, 3: diag}
+
+    def owner_cols(d):
+        return pl.ds(pl.multiple_of(((fs + d) % n) * slab, slab), slab)
+
+    def to_fs(offset):
+        return {"fs": (fs + offset + n) % n}
+
+    barrier = pltpu.get_barrier_semaphore()
+    for offset in range(1, n):
+        pl.semaphore_signal(barrier, inc=1, device_id=to_fs(offset), device_id_type=MESH)
+    for k in (1, 2, 3):
+        pl.semaphore_signal(barrier, inc=1, device_id={"tp": peers[k]}, device_id_type=MESH)
+    pl.semaphore_signal(barrier, inc=1, device_id={"rep": 1 - rep}, device_id_type=MESH)
+    pl.semaphore_wait(barrier, n - 1 + 4)
+
+    WI, WO, GU, DN = range(4)
+
+    def slot(t, d):
+        if t == WI:
+            return wi_in if d == 0 else wi_all.at[0, d]
+        if t == WO:
+            return wo_in if d == 0 else wo_all.at[0, d]
+        if t == GU:
+            return gu_in if d == 0 else gu_buf.at[d - 1]
+        return dn_in if d == 0 else dn_buf.at[d - 1]
+
+    def piece(t, d, q):
+        ref = slot(t, d)
+        rows = ref.shape[0] // QUARTERS
+        at = q + rep * (QUARTERS - 1 - 2 * q)
+        return ref.at[pl.ds(pl.multiple_of(at * rows, rows), rows), :]
+
+    def via(d, q):
+        if d == n // 2:
+            return (1, -1, 0, 0)[q]
+        if q == QUARTERS - 1:
+            return 0
+        return 1 if d < n // 2 else -1
+
+    started = []
+
+    def ring_copy(t, d, q):
+        way = via(d, q)
+        if way == 0:
+            src, dev = piece(t, d, QUARTERS - 1 - q), {"rep": 1 - rep}
+            dst = piece(t, d, QUARTERS - 1 - q)
+        else:
+            src, dev = piece(t, (d - way) % n, q), to_fs(-way)
+            dst = piece(t, d, q)
+        return pltpu.make_async_remote_copy(
+            src_ref=src, dst_ref=dst, send_sem=ring_send.at[t, d - 1, q], recv_sem=ring_recv.at[t, d - 1, q],
+            device_id=dev, device_id_type=MESH,
+        )
+
+    def send(t, d, q):
+        copy = ring_copy(t, d, q)
+        copy.start()
+        started.append(copy)
+
+    def arrived(t, d, q):
+        here = piece(t, d, q)
+        pltpu.make_async_remote_copy(
+            src_ref=here, dst_ref=here, send_sem=ring_send.at[t, d - 1, q], recv_sem=ring_recv.at[t, d - 1, q],
+            device_id=to_fs(1), device_id_type=MESH,
+        ).wait_recv()
+
+    def remote(src, dst, s_sem, r_sem, dev):
+        copy = pltpu.make_async_remote_copy(
+            src_ref=src, dst_ref=dst, send_sem=s_sem, recv_sem=r_sem, device_id=dev, device_id_type=MESH
+        )
+        copy.start()
+        started.append(copy)
+        return copy
+
+    def landed(dst, s_sem, r_sem):
+        pltpu.make_async_remote_copy(
+            src_ref=dst, dst_ref=dst, send_sem=s_sem, recv_sem=r_sem, device_id={"tp": mate}, device_id_type=MESH
+        ).wait_recv()
+
+    def send_own(t):
+        for q in range(QUARTERS - 1):
+            send(t, 1, q)
+            send(t, n - 1, q)
+
+    def relay_near(t):
+        arrived(t, 1, 0)
+        send(t, 2, 0)
+        send(t, 1, 3)
+        arrived(t, n - 1, 0)
+        send(t, n - 1, 3)
+        arrived(t, n - 1, 1)
+        send(t, 2, 1)
+
+    def relay_far(t):
+        arrived(t, 2, 0)
+        send(t, 2, 3)
+        arrived(t, 2, 1)
+        send(t, 2, 2)
+
+    def near_rest(t, d):
+        for q in ((1, 2, 3) if d == 1 else (2, 3)):
+            arrived(t, d, q)
+
+    def far_rest(t):
+        arrived(t, 2, 2)
+        arrived(t, 2, 3)
+
+    send_own(WI)
+    send_own(WO)
+    send_own(GU)
+    for offset in range(1, n):
+        remote(sc_in, sc_all.at[n - offset - 1], sc_send.at[n - offset - 1], sc_recv.at[n - offset - 1], to_fs(offset))
+    for k in (1, 2, 3):
+        remote(ps_in, ps_all.at[k - 1], tp_send.at[2, k - 1], tp_recv.at[2, k - 1], {"tp": peers[k]})
+    own_wi = pltpu.make_async_copy(wi_in, wi_all.at[0, 0], loc.at[0])
+    own_wo = pltpu.make_async_copy(wo_in, wo_all.at[0, 0], loc.at[1])
+    own_wi.start()
+    own_wo.start()
+
+    def normed_rows(values, gain):
+        mean_sq = jnp.mean(values * values, axis=-1, keepdims=True)
+        return (values * lax.rsqrt(mean_sq + eps) * gain).astype(bf16)
+
+    stage[:, 0:halo, :] = jnp.zeros((n, halo, slab), bf16)
+
+    @pl.loop(0, seq // 32)
+    def _(i):
+        rows = pl.ds(pl.multiple_of(i * 32, 32), 32)
+        first[rows, :] = normed_rows(tok[rows, :].astype(f32), gains[0:1, :])
+
+    def dot(a, b):
+        return jnp.dot(a, b, preferred_element_type=f32)
+
+    def gate_up(d, fresh):
+        weights = slot(GU, d)
+        cols = owner_cols(d)
+
+        @pl.loop(0, weights.shape[1] // TILE)
+        def _(j):
+            at = pl.ds(pl.multiple_of(j * TILE, TILE), TILE)
+            term = dot(first[:, cols], weights[:, at])
+            if fresh:
+                gacc[:, at] = term
+            else:
+                gacc[:, at] += term
+
+    def activate(gate, upper, at):
+        gate = gate * hs[0:1, at]
+        upper = upper * hs[1:2, at]
+        return (gate / (1.0 + jnp.exp(-gate)) * upper).astype(bf16)
+
+    def down(d, top):
+        weights = slot(DN, d)
+
+        @pl.loop(0, slab // TILE)
+        def _(j):
+            at = pl.ds(pl.multiple_of(j * TILE, TILE), TILE)
+            stage[d, top:top + seq, at] = dot(hidden[...], weights[:, at]).astype(bf16)
+
+    gate_up(0, True)
+    relay_near(WI)
+    relay_near(WO)
+    relay_near(GU)
+    send_own(DN)
+    relay_far(WI)
+    relay_far(WO)
+    for t in (WI, WO):
+        near_rest(t, 1)
+        near_rest(t, n - 1)
+        far_rest(t)
+    own_wi.wait()
+    own_wo.wait()
+    for k in (1, 2, 3):
+        remote(wi_all.at[0], wi_all.at[k], tp_send.at[0, k - 1], tp_recv.at[0, k - 1], {"tp": peers[k]})
+        remote(wo_all.at[0], wo_all.at[k], tp_send.at[1, k - 1], tp_recv.at[1, k - 1], {"tp": peers[k]})
+    near_rest(GU, 1)
+    gate_up(1, False)
+    near_rest(GU, n - 1)
+    gate_up(n - 1, False)
+    relay_far(GU)
+    relay_near(DN)
+    far_rest(GU)
+    gate_up(2, False)
+
+    @pl.loop(0, units // TILE)
+    def _(j):
+        at = pl.ds(pl.multiple_of(j * TILE, TILE), TILE)
+        up_at = pl.ds(pl.multiple_of(units + j * TILE, TILE), TILE)
+        hidden[:, at] = activate(gacc[:, at], gacc[:, up_at], at)
+
+    def scatter_one(d):
+        down(d, halo)
+        for k in (2, 3, 1):
+            rows = pl.ds(pl.multiple_of(peers[k] * share, share), share + halo)
+            remote(stage.at[d, rows, :], rs.at[d, k - 1], rs_send.at[d, k - 1], rs_recv.at[d, k - 1], {"tp": peers[k]})
+
+    scatter_one(0)
+    near_rest(DN, 1)
+    scatter_one(1)
+    near_rest(DN, n - 1)
+    scatter_one(n - 1)
+    relay_far(DN)
+    for d in range(1, n):
+        landed(sc_all.at[d - 1], sc_send.at[d - 1], sc_recv.at[d - 1])
+
+    def scales(d):
+        return sc_in if d == 0 else sc_all.at[d - 1]
+
+    own_window = pl.ds(pl.multiple_of(me * share, share), share + halo)
+    own_rows = pl.ds(pl.multiple_of(me * share, share), share)
+    before = pl.ds(pl.multiple_of((me * share + seq - halo) % seq, halo), halo)
+
+    def gather_one(d):
+        total = stage[d, own_window, :].astype(f32)
+        for k in (1, 2, 3):
+            landed(rs.at[d, k - 1], rs_send.at[d, k - 1], rs_recv.at[d, k - 1])
+            total = total + rs[d, k - 1].astype(f32)
+        total = 0.5 * (total * scales(d)[0:1, :])
+        cols = owner_cols(d)
+        r1[0:halo, cols] = total[0:halo] + jnp.where(me > 0, tok[before, cols].astype(f32), 0.0)
+        r1[halo:, cols] = total[halo:] + tok[own_rows, cols].astype(f32)
+
+    gather_one(0)
+    gather_one(1)
+    gather_one(n - 1)
+    far_rest(DN)
+    scatter_one(2)
+    for t in (0, 1, 2):
+        for k in (1, 2, 3):
+            where = (wi_all.at[k], wo_all.at[k], ps_all.at[k - 1])[t]
+            landed(where, tp_send.at[t, k - 1], tp_recv.at[t, k - 1])
+    gather_one(2)
+
+    second[...] = normed_rows(r1[...], gains[1:2, :])
+    for k in range(4):
+        group = me if k == 0 else peers[k]
+        total = dot(second[:, owner_cols(0)], wi_all[k, 0])
+        for d in range(1, n):
+            total = total + dot(second[:, owner_cols(d)], wi_all[k, d])
+        values = (total * isc[pl.ds(group, 1), :]).astype(bf16).astype(f32)
+        sum2 = values + pltpu.roll(values, 1, 0)
+        sum4 = sum2 + pltpu.roll(sum2, 2, 0)
+        sum8 = sum4 + pltpu.roll(sum4, 4, 0)
+        sum16 = sum8 + pltpu.roll(sum8, 8, 0)
+        summed = jnp.where(group == 0, sum2, jnp.where(group == 1, sum4, jnp.where(group == 2, sum8, sum16)))
+        span = jnp.where(group == 0, 2, jnp.where(group == 1, 4, jnp.where(group == 2, 8, 16)))
+        position = lax.broadcasted_iota(jnp.int32, (share, gc), 0) + me * share
+        counts = jnp.minimum(position + 1, span).astype(f32)
+        pooled = (summed[halo:] / counts - values[halo:]).astype(bf16)
+        pscale = (ps_in if k == 0 else ps_all.at[k - 1])[0:1, :]
+        pool[k] = (dot(pooled, pmap[group]) * pscale).astype(bf16)
+    for d in range(n):
+        cols = owner_cols(d)
+        total = dot(pool[0], wo_all[0, d])
+        for k in range(1, 4):
+            total = total + dot(pool[k], wo_all[k, d])
+        r2[:, cols] = r1[halo:, cols] + total * scales(d)[1:2, :]
+    third[own_rows, :] = normed_rows(r2[...], gains[2:3, :])
+
+    def rows_of(rank, count=1):
+        return pl.ds(pl.multiple_of(rank * share, share), share * count)
+
+    def gather_rows(ref, cols, s):
+        mine = ref.at[rows_of(me), cols]
+        remote(mine, mine, ag_send.at[s, 1], ag_recv.at[s, 1], {"tp": across})
+        remote(mine, mine, ag_send.at[s, 0], ag_recv.at[s, 0], {"tp": mate})
+
+    def forward_rows(ref, cols, s):
+        theirs = ref.at[rows_of(across), cols]
+        landed(theirs, ag_send.at[s, 1], ag_recv.at[s, 1])
+        remote(theirs, theirs, ag_send.at[s, 2], ag_recv.at[s, 2], {"tp": mate})
+
+    everything = slice(None)
+    gather_rows(third, everything, n)
+    landed(third.at[rows_of(mate), :], ag_send.at[n, 0], ag_recv.at[n, 0])
+
+    def hidden_half(chip):
+        rows = rows_of(2 * chip, 2)
+
+        @pl.loop(0, units // TILE)
+        def _(j):
+            at = pl.ds(pl.multiple_of(j * TILE, TILE), TILE)
+            up_at = pl.ds(pl.multiple_of(units + j * TILE, TILE), TILE)
+            gate = upper = None
+            for d in range(n):
+                weights = slot(GU, d)
+                left = third[rows, owner_cols(d)]
+                g, u = dot(left, weights[:, at]), dot(left, weights[:, up_at])
+                gate, upper = (g, u) if gate is None else (gate + g, upper + u)
+            hidden[rows, at] = activate(gate, upper, at)
+
+    for copy in started:
+        copy.wait_send()
+    started.clear()
+    forward_rows(third, everything, n)
+    hidden_half(me // 2)
+    landed(third.at[rows_of(diag), :], ag_send.at[n, 2], ag_recv.at[n, 2])
+    hidden_half(1 - me // 2)
+    for d in range(n):
+        down(d, 0)
+        remote(stage.at[d, rows_of(diag), :], rs_a.at[d, 1], rs_send.at[n + d, 1], rs_recv.at[n + d, 1], {"tp": mate})
+        remote(stage.at[d, rows_of(mate), :], rs_a.at[d, 0], rs_send.at[n + d, 0], rs_recv.at[n + d, 0], {"tp": mate})
+    for d in range(n):
+        landed(rs_a.at[d, 1], rs_send.at[n + d, 1], rs_recv.at[n + d, 1])
+        s_b[d] = (stage[d, rows_of(across), :].astype(f32) + rs_a[d, 1].astype(f32)).astype(bf16)
+        remote(s_b.at[d], rs_b.at[d], rs_send.at[n + d, 2], rs_recv.at[n + d, 2], {"tp": across})
+    for d in range(n):
+        landed(rs_a.at[d, 0], rs_send.at[n + d, 0], rs_recv.at[n + d, 0])
+        landed(rs_b.at[d], rs_send.at[n + d, 2], rs_recv.at[n + d, 2])
+        total = stage[d, rows_of(me), :].astype(f32) + rs_a[d, 0].astype(f32) + rs_b[d].astype(f32)
+        cols = owner_cols(d)
+        out[rows_of(me), cols] = (r2[:, cols] + 0.5 * (total * scales(d)[0:1, :])).astype(bf16)
+        gather_rows(out, cols, d)
+    for d in range(n):
+        forward_rows(out, owner_cols(d), d)
+    for d in range(n):
+        landed(out.at[rows_of(mate), owner_cols(d)], ag_send.at[d, 0], ag_recv.at[d, 0])
+        landed(out.at[rows_of(diag), owner_cols(d)], ag_send.at[d, 2], ag_recv.at[d, 2])
+    for copy in started:
+        copy.wait_send()
+
+
+def fused_layer(
+    tokens, norm_gains, gate_weight, up_weight, hidden_scales, down_weight, down_scale, mix_in, in_scale,
+    pool_map, pool_scale, mix_out, out_scale,
+):
+    n = lax.axis_size("fs")
+    seq, width = tokens.shape
+    slab, units = gate_weight.shape
+    groups, gc, _ = pool_map.shape
+    share = seq // 4
+    padded = share + widest
+    rank = lax.axis_index("tp")
+    gate_up_in = jnp.concatenate([gate_weight.astype(bf16), up_weight.astype(bf16)], axis=1)
+    down_in = down_weight.astype(bf16)
+    in_cols = lax.dynamic_slice_in_dim(mix_in, rank * gc, gc, 1).astype(bf16)
+    out_rows = mix_out.astype(bf16)
+    own_scales = jnp.concatenate([down_scale[None], out_scale[None], jnp.zeros((6, slab), f32)], axis=0)
+    own_pool = jnp.broadcast_to(pool_scale[None], (8, gc))
+    vmem = pl.BlockSpec(memory_space=pltpu.VMEM)
+    dma = pltpu.SemaphoreType.DMA
+    args = (
+        tokens, norm_gains, gate_up_in, hidden_scales, down_in, in_cols, out_rows, in_scale.reshape(groups, gc),
+        pool_map.astype(bf16), own_pool, own_scales,
+    )
+    return pl.pallas_call(
+        functools.partial(layer_kernel, n),
+        out_shape=jax.ShapeDtypeStruct((seq, width), bf16),
+        in_specs=[vmem] * len(args),
+        out_specs=vmem,
+        scratch_shapes=[
+            pltpu.VMEM((n - 1, slab, 2 * units), bf16),
+            pltpu.VMEM((n - 1, units, slab), bf16),
+            pltpu.VMEM((4, n, slab, gc), bf16),
+            pltpu.VMEM((4, n, gc, slab), bf16),
+            pltpu.VMEM((n - 1, 8, slab), f32),
+            pltpu.VMEM((3, 8, gc), f32),
+            pltpu.VMEM((seq, width), bf16),
+            pltpu.VMEM((seq, 2 * units), f32),
+            pltpu.VMEM((seq, units), bf16),
+            pltpu.VMEM((n, seq + widest, slab), bf16),
+            pltpu.VMEM((n, 3, padded, slab), bf16),
+            pltpu.VMEM((padded, width), f32),
+            pltpu.VMEM((padded, width), bf16),
+            pltpu.VMEM((4, share, gc), bf16),
+            pltpu.VMEM((share, width), f32),
+            pltpu.VMEM((seq, width), bf16),
+            pltpu.VMEM((n, 2, share, slab), bf16),
+            pltpu.VMEM((n, share, slab), bf16),
+            pltpu.VMEM((n, share, slab), bf16),
+            dma((4, n - 1, QUARTERS)), dma((4, n - 1, QUARTERS)),
+            dma((n - 1,)), dma((n - 1,)),
+            dma((3, 3)), dma((3, 3)),
+            dma((2 * n, 3)), dma((2 * n, 3)),
+            dma((n + 1, 3)), dma((n + 1, 3)),
+            dma((2,)),
+        ],
+        compiler_params=pltpu.CompilerParams(
+            collective_id=0, has_side_effects=True, vmem_limit_bytes=60 * 1024 * 1024
+        ),
+    )(*args)
+
+
 def solution(mesh):
+    body = fused_layer if fits_kernel(mesh) else per_device
     return jax.shard_map(
-        per_device,
+        body,
         mesh=mesh,
         in_specs=(
             P(("rep", "fs"), None),

time: 380 us -> 183 us (0.48)
  waiting for transfers between devices: 267 us -> 0 us
  Pallas kernels: 0 us -> 169 us
  blocking collectives: 55.9 us -> 0 us
  matrix products: 23.9 us -> 0 us
  between operations: 13.4 us -> 0.04 us
  other arithmetic: 16.1 us -> 8.57 us
    all_gather x6 -> x0, waiting for transfers between devices: 218 us -> none  [the longest x1 63.7 us: per_device(): lax.all_gather(up_bf, 'fs', axis=0, tiled=True)]
    pallas_call x0 -> x1, Pallas kernels: none -> 169 us  [fused_layer(): pl.pallas_call(functools.partial(layer_kernel, n), out_shape=jax.ShapeDty...]
    all_gather x4 -> x0, blocking collectives: 55.9 us -> none  [the longest x1 16.2 us: fetch_mixer(): lax.all_gather(in_cols.astype(jnp.bfloat16), 'fs', axis=0, tiled=True)]
    reduce_scatter x3 -> x0, waiting for transfers between devices: 48.3 us -> none  [scatter_rows(): lax.psum_scatter(term_fn(jnp.int32(0), lax.axis_size('tp') * share).astyp...]
    dot_general x6 -> x0, matrix products: 23.9 us -> none  [the longest x2 12.6 us: term_rows(): return jnp.dot(hidden, down_full, preferred_element_type=jnp.float32)]
    convert_element_type x8 -> x5, other arithmetic: 13.2 us -> 5.9 us  [the longest x1 1.74 us: fused_layer(): pool_map.astype(bf16)]
  transfers between devices with their start and end apart: 9 -> 0, of which waited for: 8 -> 0; matrix products, arithmetic and copies ran while one was open for 3% -> 0% of each run, Pallas kernels for 0% -> 0%
where the time goes in v1:
time: 183 us
  Pallas kernels  169 us (92%)
  other arithmetic  8.57 us (5%)
  local copies, waits for them, and re-layouts  5.09 us (3%)
    pallas_call x1, Pallas kernels, fused_layer(): pl.pallas_call(functools.partial(layer_kernel, n), out_shape=jax.ShapeDty...  169 us

profile of v1, /device:TPU:0, one launch (start us, length us, event | category | flops | bytes accessed | tf_op | source)
XLA Modules:
  0.0 182.9 jit_solution(13824773687230200237)
XLA Ops:
  0.0 0.0 copy-start
  0.0 0.1 pad.2.clone
  0.1 1.3 broadcast_in_dim.15.ps_in
  1.4 1.4 maximum_maximum_fusion.sc_in
  2.8 0.0 copy-done
  2.8 0.7 dynamic-slice_convert_fusion.wi_in
  3.5 0.0 copy-start.1
  3.5 1.7 convert_element_type.23.pmap
  5.2 1.6 convert_element_type.22.wo_in
  6.8 1.5 convert_element_type.18
  8.3 0.0 copy-done.1
  8.3 0.1 convert_element_type.19
  8.4 0.0 copy-start.2
  8.4 1.3 pad_maximum_fusion.gu_in
  9.7 0.7 copy-done.2
  10.4 1.0 convert_element_type.20.dn_in
  11.4 169.2 %shard_map.127 = bf16[256,2048]{1,0:T(8,128)(2,1)} custom-call(bf16[256,2048]{1,0:T(8,128)(2,1)} %tok.1, f32[3,2048]{1,0:T(4,128)} %gains.1, bf16[512,1536]{1,0:T(8,128)(2,1)} %pad_maximum_fusion.gu_in, f32[2,768]{1,0:T(2,128)} %hs.1, bf16[768,512]{1,0:T(8,128)(2,1)} %convert_element_type.20.dn_in, bf16[512,128]{1,0:T(8,128)(2,1)} %dynamic-slice_convert_fusion.wi_in, ...), custom_call_target="tpu_custom_call" | custom-call | tf_op jit(solution)/shard_map/pallas_call | solution.py:517
  180.6 2.3 %copy.15 = bf16[256,2048]{1,0:T(8,128)(2,1)} copy(bf16[256,2048]{1,0:T(8,128)(2,1)} %shard_map.127) | data formatting | bytes 2097152
  (1 shorter events, 0.0 us)
Async XLA Ops:
  0.0 2.8 %copy-start = (f32[512,512]{1,0:T(8,128)S(1)}, f32[512,512]{1,0:T(8,128)}, u32[]{:S(2)}) copy-start(f32[512,512]{1,0:T(8,128)} %param.20) | copy-start | bytes 3145732
  3.5 4.9 %copy-start.1 = (f32[512,768]{1,0:T(8,128)S(1)}, f32[512,768]{1,0:T(8,128)}, u32[]{:S(2)}) copy-start(f32[512,768]{1,0:T(8,128)} %param.16) | copy-start | bytes 4718596
  8.4 2.0 %copy-start.2 = (f32[768,512]{1,0:T(8,128)S(1)}, f32[768,512]{1,0:T(8,128)}, u32[]{:S(2)}) copy-start(f32[768,512]{1,0:T(8,128)} %param.18) | copy-start | bytes 4718596

commit v2 on v1

--- a/solution.py
+++ b/solution.py
@@ -151,8 +151,8 @@
 
 
 def layer_kernel(
-    n, tok, gains, gu_in, hs, dn_in, wi_in, wo_in, isc, pmap, ps_in, sc_in,
-    out, gu_buf, dn_buf, wi_all, wo_all, sc_all, ps_all,
+    n, tok, gains, gate_hbm, up_hbm, hs, down_hbm, mix_in_hbm, mix_out_hbm, isc, pmap, pool_scale, down_scale, out_scale,
+    out, gu_in, dn_in, wi_in, wo_in, wide_gate, wide_up, wide_down, wide_in, wide_out, sc_in, ps_in, gu_buf, dn_buf, wi_all, wo_all, sc_all, ps_all,
     first, gacc, hidden, stage, rs, r1, second, pool, r2, third, rs_a, s_b, rs_b,
     ring_send, ring_recv, sc_send, sc_recv, tp_send, tp_recv, rs_send, rs_recv, ag_send, ag_recv, loc,
 ):
@@ -170,11 +170,33 @@
     diag = (mate + 2) % 4
     peers = {1: mate, 2: across, 3: diag}
 
-    def owner_cols(d):
-        return pl.ds(pl.multiple_of(((fs + d) % n) * slab, slab), slab)
+    order = (
+        fs,
+        jnp.where(fs == 0, 1, fs - 1),
+        jnp.where(fs == 0, 2, jnp.where(fs == 1, 2, jnp.where(fs == 2, 3, 1))),
+        jnp.where(fs < 2, 3, 0),
+    )
+
+    def owner_cols(i):
+        return pl.ds(pl.multiple_of(order[i] * slab, slab), slab)
 
     def to_fs(offset):
         return {"fs": (fs + offset + n) % n}
+
+    columns_in = pl.ds(pl.multiple_of(me * gc, gc), gc)
+    loads = [
+        pltpu.make_async_copy(mix_in_hbm.at[:, columns_in], wide_in, loc.at[2]),
+        pltpu.make_async_copy(mix_out_hbm, wide_out, loc.at[3]),
+        pltpu.make_async_copy(gate_hbm, wide_gate, loc.at[4]),
+        pltpu.make_async_copy(up_hbm, wide_up, loc.at[5]),
+        pltpu.make_async_copy(down_hbm, wide_down, loc.at[6]),
+    ]
+    for load in loads:
+        load.start()
+    sc_in[...] = jnp.zeros_like(sc_in)
+    sc_in[0:1, :] = down_scale[...]
+    sc_in[1:2, :] = out_scale[...]
+    ps_in[...] = jnp.broadcast_to(pool_scale[...], ps_in.shape)
 
     barrier = pltpu.get_barrier_semaphore()
     for offset in range(1, n):
@@ -182,66 +204,72 @@
     for k in (1, 2, 3):
         pl.semaphore_signal(barrier, inc=1, device_id={"tp": peers[k]}, device_id_type=MESH)
     pl.semaphore_signal(barrier, inc=1, device_id={"rep": 1 - rep}, device_id_type=MESH)
-    pl.semaphore_wait(barrier, n - 1 + 4)
 
     WI, WO, GU, DN = range(4)
 
-    def slot(t, d):
+    def slot(t, i):
         if t == WI:
-            return wi_in if d == 0 else wi_all.at[0, d]
+            return wi_in if i == 0 else wi_all.at[0, order[i]]
         if t == WO:
-            return wo_in if d == 0 else wo_all.at[0, d]
+            return wo_in if i == 0 else wo_all.at[0, order[i]]
         if t == GU:
-            return gu_in if d == 0 else gu_buf.at[d - 1]
-        return dn_in if d == 0 else dn_buf.at[d - 1]
-
-    def piece(t, d, q):
-        ref = slot(t, d)
+            return gu_in if i == 0 else gu_buf.at[order[i]]
+        return dn_in if i == 0 else dn_buf.at[order[i]]
+
+    def there(t):
+        return (wi_all.at[0], wo_all.at[0], gu_buf, dn_buf)[t]
+
+    def quarter(ref, at):
         rows = ref.shape[0] // QUARTERS
-        at = q + rep * (QUARTERS - 1 - 2 * q)
         return ref.at[pl.ds(pl.multiple_of(at * rows, rows), rows), :]
 
-    def via(d, q):
-        if d == n // 2:
-            return (1, -1, 0, 0)[q]
-        if q == QUARTERS - 1:
-            return 0
-        return 1 if d < n // 2 else -1
-
     started = []
 
-    def ring_copy(t, d, q):
-        way = via(d, q)
-        if way == 0:
-            src, dev = piece(t, d, QUARTERS - 1 - q), {"rep": 1 - rep}
-            dst = piece(t, d, QUARTERS - 1 - q)
+    def start_if(cond, copy):
+        if cond is None:
+            copy.start()
         else:
-            src, dev = piece(t, (d - way) % n, q), to_fs(-way)
-            dst = piece(t, d, q)
-        return pltpu.make_async_remote_copy(
-            src_ref=src, dst_ref=dst, send_sem=ring_send.at[t, d - 1, q], recv_sem=ring_recv.at[t, d - 1, q],
+            @pl.when(cond)
+            def _():
+                copy.start()
+        started.append((cond, copy))
+
+    def wait_sent():
+        for cond, copy in started:
+            if cond is None:
+                copy.wait_send()
+            else:
+                @pl.when(cond)
+                def _():
+                    copy.wait_send()
+        started.clear()
+
+    UP, BACK, REP = range(3)
+
+    def send(t, i, u, way):
+        at = rep * 2 + u
+        shard = order[i]
+        dev = (to_fs(1), to_fs(-1), {"rep": 1 - rep})[way]
+        cond = (fs < n - 1, fs > 0, None)[way]
+        if i > 0 and way != REP:
+            cond = cond & ((shard < fs) if way == UP else (shard > fs))
+        start_if(cond, pltpu.make_async_remote_copy(
+            src_ref=quarter(slot(t, i), at), dst_ref=quarter(there(t).at[shard], at),
+            send_sem=ring_send.at[way, t, i, u], recv_sem=ring_recv.at[t, shard, at],
             device_id=dev, device_id_type=MESH,
-        )
-
-    def send(t, d, q):
-        copy = ring_copy(t, d, q)
-        copy.start()
-        started.append(copy)
-
-    def arrived(t, d, q):
-        here = piece(t, d, q)
+        ))
+
+    def arrived(t, i, at):
+        here = quarter(slot(t, i), at)
         pltpu.make_async_remote_copy(
-            src_ref=here, dst_ref=here, send_sem=ring_send.at[t, d - 1, q], recv_sem=ring_recv.at[t, d - 1, q],
-            device_id=to_fs(1), device_id_type=MESH,
+            src_ref=here, dst_ref=here, send_sem=ring_send.at[0, t, i, 0], recv_sem=ring_recv.at[t, order[i], at],
+            device_id={"rep": 1 - rep}, device_id_type=MESH,
         ).wait_recv()
 
     def remote(src, dst, s_sem, r_sem, dev):
-        copy = pltpu.make_async_remote_copy(
+        start_if(None, pltpu.make_async_remote_copy(
             src_ref=src, dst_ref=dst, send_sem=s_sem, recv_sem=r_sem, device_id=dev, device_id_type=MESH
-        )
-        copy.start()
-        started.append(copy)
-        return copy
+        ))
 
     def landed(dst, s_sem, r_sem):
         pltpu.make_async_remote_copy(
@@ -249,42 +277,51 @@
         ).wait_recv()
 
     def send_own(t):
-        for q in range(QUARTERS - 1):
-            send(t, 1, q)
-            send(t, n - 1, q)
-
-    def relay_near(t):
-        arrived(t, 1, 0)
-        send(t, 2, 0)
-        send(t, 1, 3)
-        arrived(t, n - 1, 0)
-        send(t, n - 1, 3)
-        arrived(t, n - 1, 1)
-        send(t, 2, 1)
-
-    def relay_far(t):
-        arrived(t, 2, 0)
-        send(t, 2, 3)
-        arrived(t, 2, 1)
-        send(t, 2, 2)
-
-    def near_rest(t, d):
-        for q in ((1, 2, 3) if d == 1 else (2, 3)):
-            arrived(t, d, q)
-
-    def far_rest(t):
-        arrived(t, 2, 2)
-        arrived(t, 2, 3)
-
+        for u in range(2):
+            send(t, 0, u, UP)
+            send(t, 0, u, BACK)
+
+    def relay(t, i):
+        for u in range(2):
+            arrived(t, i, rep * 2 + u)
+            send(t, i, u, UP)
+            send(t, i, u, BACK)
+            send(t, i, u, REP)
+
+    def rest(t, i):
+        for u in range(2):
+            arrived(t, i, (1 - rep) * 2 + u)
+
+    loads[0].wait()
+    loads[1].wait()
+    wi_in[...] = wide_in[...].astype(bf16)
+    wo_in[...] = wide_out[...].astype(bf16)
+    loads[2].wait()
+    loads[3].wait()
+
+    @pl.loop(0, slab // 32)
+    def _(j):
+        rows = pl.ds(pl.multiple_of(j * 32, 32), 32)
+        gu_in[rows, 0:units] = wide_gate[rows, :].astype(bf16)
+        gu_in[rows, units:] = wide_up[rows, :].astype(bf16)
+
+    pl.semaphore_wait(barrier, n - 1 + 4)
     send_own(WI)
     send_own(WO)
     send_own(GU)
+    loads[4].wait()
+
+    @pl.loop(0, units // 32)
+    def _(j):
+        rows = pl.ds(pl.multiple_of(j * 32, 32), 32)
+        dn_in[rows, :] = wide_down[rows, :].astype(bf16)
+
     for offset in range(1, n):
-        remote(sc_in, sc_all.at[n - offset - 1], sc_send.at[n - offset - 1], sc_recv.at[n - offset - 1], to_fs(offset))
+        remote(sc_in, sc_all.at[fs], sc_send.at[offset - 1], sc_recv.at[fs], to_fs(offset))
     for k in (1, 2, 3):
         remote(ps_in, ps_all.at[k - 1], tp_send.at[2, k - 1], tp_recv.at[2, k - 1], {"tp": peers[k]})
-    own_wi = pltpu.make_async_copy(wi_in, wi_all.at[0, 0], loc.at[0])
-    own_wo = pltpu.make_async_copy(wo_in, wo_all.at[0, 0], loc.at[1])
+    own_wi = pltpu.make_async_copy(wi_in, wi_all.at[0, fs], loc.at[0])
+    own_wo = pltpu.make_async_copy(wo_in, wo_all.at[0, fs], loc.at[1])
     own_wi.start()
     own_wo.start()
 
@@ -329,29 +366,28 @@
             stage[d, top:top + seq, at] = dot(hidden[...], weights[:, at]).astype(bf16)
 
     gate_up(0, True)
-    relay_near(WI)
-    relay_near(WO)
-    relay_near(GU)
+    for t in (WI, WO, GU):
+        relay(t, 1)
     send_own(DN)
-    relay_far(WI)
-    relay_far(WO)
+    for t in (WI, WO, GU):
+        relay(t, 2)
+    rest(GU, 1)
+    gate_up(1, False)
+    for t in (WI, WO, GU):
+        relay(t, 3)
+    rest(GU, 2)
+    gate_up(2, False)
     for t in (WI, WO):
-        near_rest(t, 1)
-        near_rest(t, n - 1)
-        far_rest(t)
+        for i in range(1, n):
+            rest(t, i)
     own_wi.wait()
     own_wo.wait()
     for k in (1, 2, 3):
         remote(wi_all.at[0], wi_all.at[k], tp_send.at[0, k - 1], tp_recv.at[0, k - 1], {"tp": peers[k]})
         remote(wo_all.at[0], wo_all.at[k], tp_send.at[1, k - 1], tp_recv.at[1, k - 1], {"tp": peers[k]})
-    near_rest(GU, 1)
-    gate_up(1, False)
-    near_rest(GU, n - 1)
-    gate_up(n - 1, False)
-    relay_far(GU)
-    relay_near(DN)
-    far_rest(GU)
-    gate_up(2, False)
+    relay(DN, 1)
+    rest(GU, 3)
+    gate_up(3, False)
 
     @pl.loop(0, units // TILE)
     def _(j):
@@ -365,17 +401,11 @@
             rows = pl.ds(pl.multiple_of(peers[k] * share, share), share + halo)
             remote(stage.at[d, rows, :], rs.at[d, k - 1], rs_send.at[d, k - 1], rs_recv.at[d, k - 1], {"tp": peers[k]})
 
-    scatter_one(0)
-    near_rest(DN, 1)
-    scatter_one(1)
-    near_rest(DN, n - 1)
-    scatter_one(n - 1)
-    relay_far(DN)
-    for d in range(1, n):
-        landed(sc_all.at[d - 1], sc_send.at[d - 1], sc_recv.at[d - 1])
+    for i in range(1, n):
+        landed(sc_all.at[order[i]], sc_send.at[0], sc_recv.at[order[i]])
 
     def scales(d):
-        return sc_in if d == 0 else sc_all.at[d - 1]
+        return sc_in if d == 0 else sc_all.at[order[d]]
 
     own_window = pl.ds(pl.multiple_of(me * share, share), share + halo)
     own_rows = pl.ds(pl.multiple_of(me * share, share), share)
@@ -391,23 +421,30 @@
         r1[0:halo, cols] = total[0:halo] + jnp.where(me > 0, tok[before, cols].astype(f32), 0.0)
         r1[halo:, cols] = total[halo:] + tok[own_rows, cols].astype(f32)
 
+    scatter_one(0)
+    relay(DN, 2)
+    rest(DN, 1)
+    scatter_one(1)
     gather_one(0)
+    relay(DN, 3)
+    rest(DN, 2)
+    scatter_one(2)
     gather_one(1)
-    gather_one(n - 1)
-    far_rest(DN)
-    scatter_one(2)
+    rest(DN, 3)
+    scatter_one(3)
+    gather_one(2)
     for t in (0, 1, 2):
         for k in (1, 2, 3):
             where = (wi_all.at[k], wo_all.at[k], ps_all.at[k - 1])[t]
             landed(where, tp_send.at[t, k - 1], tp_recv.at[t, k - 1])
-    gather_one(2)
+    gather_one(3)
 
     second[...] = normed_rows(r1[...], gains[1:2, :])
     for k in range(4):
         group = me if k == 0 else peers[k]
-        total = dot(second[:, owner_cols(0)], wi_all[k, 0])
+        total = dot(second[:, owner_cols(0)], wi_all[k, fs])
         for d in range(1, n):
-            total = total + dot(second[:, owner_cols(d)], wi_all[k, d])
+            total = total + dot(second[:, owner_cols(d)], wi_all[k, order[d]])
         values = (total * isc[pl.ds(group, 1), :]).astype(bf16).astype(f32)
         sum2 = values + pltpu.roll(values, 1, 0)
         sum4 = sum2 + pltpu.roll(sum2, 2, 0)
@@ -419,12 +456,12 @@
         counts = jnp.minimum(position + 1, span).astype(f32)
         pooled = (summed[halo:] / counts - values[halo:]).astype(bf16)
         pscale = (ps_in if k == 0 else ps_all.at[k - 1])[0:1, :]
-        pool[k] = (dot(pooled, pmap[group]) * pscale).astype(bf16)
+        pool[k] = (dot(pooled, pmap[group].astype(bf16)) * pscale).astype(bf16)
     for d in range(n):
         cols = owner_cols(d)
-        total = dot(pool[0], wo_all[0, d])
+        total = dot(pool[0], wo_all[0, order[d]])
         for k in range(1, 4):
-            total = total + dot(pool[k], wo_all[k, d])
+            total = total + dot(pool[k], wo_all[k, order[d]])
         r2[:, cols] = r1[halo:, cols] + total * scales(d)[1:2, :]
     third[own_rows, :] = normed_rows(r2[...], gains[2:3, :])
 
@@ -460,9 +497,7 @@
                 gate, upper = (g, u) if gate is None else (gate + g, upper + u)
             hidden[rows, at] = activate(gate, upper, at)
 
-    for copy in started:
-        copy.wait_send()
-    started.clear()
+    wait_sent()
     forward_rows(third, everything, n)
     hidden_half(me // 2)
     landed(third.at[rows_of(diag), :], ag_send.at[n, 2], ag_recv.at[n, 2])
@@ -487,8 +522,7 @@
     for d in range(n):
         landed(out.at[rows_of(mate), owner_cols(d)], ag_send.at[d, 0], ag_recv.at[d, 0])
         landed(out.at[rows_of(diag), owner_cols(d)], ag_send.at[d, 2], ag_recv.at[d, 2])
-    for copy in started:
-        copy.wait_send()
+    wait_sent()
 
 
 def fused_layer(
@@ -501,30 +535,36 @@
     groups, gc, _ = pool_map.shape
     share = seq // 4
     padded = share + widest
-    rank = lax.axis_index("tp")
-    gate_up_in = jnp.concatenate([gate_weight.astype(bf16), up_weight.astype(bf16)], axis=1)
-    down_in = down_weight.astype(bf16)
-    in_cols = lax.dynamic_slice_in_dim(mix_in, rank * gc, gc, 1).astype(bf16)
-    out_rows = mix_out.astype(bf16)
-    own_scales = jnp.concatenate([down_scale[None], out_scale[None], jnp.zeros((6, slab), f32)], axis=0)
-    own_pool = jnp.broadcast_to(pool_scale[None], (8, gc))
     vmem = pl.BlockSpec(memory_space=pltpu.VMEM)
     dma = pltpu.SemaphoreType.DMA
+    hbm = pl.BlockSpec(memory_space=pl.ANY)
     args = (
-        tokens, norm_gains, gate_up_in, hidden_scales, down_in, in_cols, out_rows, in_scale.reshape(groups, gc),
-        pool_map.astype(bf16), own_pool, own_scales,
+        (tokens, vmem), (norm_gains, vmem), (gate_weight, hbm), (up_weight, hbm), (hidden_scales, vmem),
+        (down_weight, hbm), (mix_in, hbm), (mix_out, hbm), (in_scale.reshape(groups, gc), vmem), (pool_map, vmem),
+        (pool_scale[None], vmem), (down_scale[None], vmem), (out_scale[None], vmem),
     )
     return pl.pallas_call(
         functools.partial(layer_kernel, n),
         out_shape=jax.ShapeDtypeStruct((seq, width), bf16),
-        in_specs=[vmem] * len(args),
+        in_specs=[spec for _, spec in args],
         out_specs=vmem,
         scratch_shapes=[
-            pltpu.VMEM((n - 1, slab, 2 * units), bf16),
-            pltpu.VMEM((n - 1, units, slab), bf16),
+            pltpu.VMEM((slab, 2 * units), bf16),
+            pltpu.VMEM((units, slab), bf16),
+            pltpu.VMEM((slab, gc), bf16),
+            pltpu.VMEM((gc, slab), bf16),
+            pltpu.VMEM((slab, units), f32),
+            pltpu.VMEM((slab, units), f32),
+            pltpu.VMEM((units, slab), f32),
+            pltpu.VMEM((slab, gc), f32),
+            pltpu.VMEM((gc, slab), f32),
+            pltpu.VMEM((8, slab), f32),
+            pltpu.VMEM((8, gc), f32),
+            pltpu.VMEM((n, slab, 2 * units), bf16),
+            pltpu.VMEM((n, units, slab), bf16),
             pltpu.VMEM((4, n, slab, gc), bf16),
             pltpu.VMEM((4, n, gc, slab), bf16),
-            pltpu.VMEM((n - 1, 8, slab), f32),
+            pltpu.VMEM((n, 8, slab), f32),
             pltpu.VMEM((3, 8, gc), f32),
             pltpu.VMEM((seq, width), bf16),
             pltpu.VMEM((seq, 2 * units), f32),
@@ -539,17 +579,17 @@
             pltpu.VMEM((n, 2, share, slab), bf16),
             pltpu.VMEM((n, share, slab), bf16),
             pltpu.VMEM((n, share, slab), bf16),
-            dma((4, n - 1, QUARTERS)), dma((4, n - 1, QUARTERS)),
-            dma((n - 1,)), dma((n - 1,)),
+            dma((3, 4, n, 2)), dma((4, n, QUARTERS)),
+            dma((n - 1,)), dma((n,)),
             dma((3, 3)), dma((3, 3)),
             dma((2 * n, 3)), dma((2 * n, 3)),
             dma((n + 1, 3)), dma((n + 1, 3)),
-            dma((2,)),
+            dma((7,)),
         ],
         compiler_params=pltpu.CompilerParams(
             collective_id=0, has_side_effects=True, vmem_limit_bytes=60 * 1024 * 1024
         ),
-    )(*args)
+    )(*[value for value, _ in args])
 
 
 def solution(mesh):

time: 183 us -> 179 us (0.978)
  other arithmetic: 8.57 us -> 0 us
  Pallas kernels: 169 us -> 176 us
  local copies, waits for them, and re-layouts: 5.09 us -> 2.3 us
    pallas_call x1, Pallas kernels: 169 us -> 176 us  [fused_layer(): pl.pallas_call(functools.partial(layer_kernel, n), out_shape=jax.ShapeDty...]
    convert_element_type x5 -> x0, other arithmetic: 5.9 us -> none  [the longest x1 1.74 us: fused_layer(): pool_map.astype(bf16)]
    concatenate x2 -> x0, other arithmetic: 2.67 us -> none  [the longest x1 1.38 us: fused_layer(): jnp.concatenate([down_scale[None], out_scale[None], jnp.zeros((6, slab),...]
where the time goes in v2:
time: 179 us
  Pallas kernels  176 us (98%)
  local copies, waits for them, and re-layouts  2.3 us (1%)
    pallas_call x1, Pallas kernels, fused_layer(): pl.pallas_call(functools.partial(layer_kernel, n), out_shape=jax.ShapeDty...  176 us

profile of v2, /device:TPU:0, one launch (start us, length us, event | category | flops | bytes accessed | tf_op | source)
XLA Modules:
  0.0 178.8 jit_solution(4743054035734744234)
XLA Ops:
  0.0 176.4 %shard_map.127 = bf16[256,2048]{1,0:T(8,128)(2,1)} custom-call(bf16[256,2048]{1,0:T(8,128)(2,1)} %tok.1, f32[3,2048]{1,0:T(4,128)} %gains.1, f32[512,768]{1,0:T(8,128)} %gate_hbm.1, f32[512,768]{1,0:T(8,128)} %up_hbm.1, f32[2,768]{1,0:T(2,128)} %hs.1, f32[768,512]{1,0:T(8,128)} %down_hbm.1, f32[512,512]{1,0:T(8,128)} %mix_in_hbm.1, f32[128,512]{1,0:T(8,128)} %mix_out_hbm.1, ...), custom_call_target="tpu_custom_call" | custom-call | tf_op jit(solution)/shard_map/pallas_call | solution.py:546
  176.4 2.3 %copy.15 = bf16[256,2048]{1,0:T(8,128)(2,1)} copy(bf16[256,2048]{1,0:T(8,128)(2,1)} %shard_map.127) | data formatting | bytes 2097152

commit v3 on v2

--- a/solution.py
+++ b/solution.py
@@ -140,7 +140,8 @@
 
 
 MESH = pl.DeviceIdType.MESH
-QUARTERS = 4
+PARTS = (1, 1, 2, 4)
+FIRST_PART = (0, 1, 2, 4, 8)
 TILE = 256
 bf16 = jnp.bfloat16
 f32 = jnp.float32
@@ -184,26 +185,30 @@
         return {"fs": (fs + offset + n) % n}
 
     columns_in = pl.ds(pl.multiple_of(me * gc, gc), gc)
+    half = slab // 2
+    mine_half = pl.ds(pl.multiple_of(rep * half, half), half)
+    other_half = pl.ds(pl.multiple_of((1 - rep) * half, half), half)
     loads = [
         pltpu.make_async_copy(mix_in_hbm.at[:, columns_in], wide_in, loc.at[2]),
         pltpu.make_async_copy(mix_out_hbm, wide_out, loc.at[3]),
-        pltpu.make_async_copy(gate_hbm, wide_gate, loc.at[4]),
-        pltpu.make_async_copy(up_hbm, wide_up, loc.at[5]),
-        pltpu.make_async_copy(down_hbm, wide_down, loc.at[6]),
+        pltpu.make_async_copy(gate_hbm.at[mine_half, :], wide_gate.at[mine_half, :], loc.at[4]),
+        pltpu.make_async_copy(up_hbm.at[mine_half, :], wide_up.at[mine_half, :], loc.at[5]),
+        pltpu.make_async_copy(gate_hbm.at[other_half, :], wide_gate.at[other_half, :], loc.at[6]),
+        pltpu.make_async_copy(up_hbm.at[other_half, :], wide_up.at[other_half, :], loc.at[7]),
+        pltpu.make_async_copy(down_hbm, wide_down, loc.at[8]),
     ]
     for load in loads:
         load.start()
-    sc_in[...] = jnp.zeros_like(sc_in)
-    sc_in[0:1, :] = down_scale[...]
-    sc_in[1:2, :] = out_scale[...]
-    ps_in[...] = jnp.broadcast_to(pool_scale[...], ps_in.shape)
-
     barrier = pltpu.get_barrier_semaphore()
     for offset in range(1, n):
         pl.semaphore_signal(barrier, inc=1, device_id=to_fs(offset), device_id_type=MESH)
     for k in (1, 2, 3):
         pl.semaphore_signal(barrier, inc=1, device_id={"tp": peers[k]}, device_id_type=MESH)
     pl.semaphore_signal(barrier, inc=1, device_id={"rep": 1 - rep}, device_id_type=MESH)
+    sc_in[...] = jnp.zeros_like(sc_in)
+    sc_in[0:1, :] = down_scale[...]
+    sc_in[1:2, :] = out_scale[...]
+    ps_in[...] = jnp.broadcast_to(pool_scale[...], ps_in.shape)
 
     WI, WO, GU, DN = range(4)
 
@@ -219,8 +224,8 @@
     def there(t):
         return (wi_all.at[0], wo_all.at[0], gu_buf, dn_buf)[t]
 
-    def quarter(ref, at):
-        rows = ref.shape[0] // QUARTERS
+    def part_of(ref, t, at):
+        rows = ref.shape[0] // (2 * PARTS[t])
         return ref.at[pl.ds(pl.multiple_of(at * rows, rows), rows), :]
 
     started = []
@@ -247,22 +252,22 @@
     UP, BACK, REP = range(3)
 
     def send(t, i, u, way):
-        at = rep * 2 + u
+        at = rep * PARTS[t] + u
         shard = order[i]
         dev = (to_fs(1), to_fs(-1), {"rep": 1 - rep})[way]
         cond = (fs < n - 1, fs > 0, None)[way]
         if i > 0 and way != REP:
             cond = cond & ((shard < fs) if way == UP else (shard > fs))
         start_if(cond, pltpu.make_async_remote_copy(
-            src_ref=quarter(slot(t, i), at), dst_ref=quarter(there(t).at[shard], at),
-            send_sem=ring_send.at[way, t, i, u], recv_sem=ring_recv.at[t, shard, at],
+            src_ref=part_of(slot(t, i), t, at), dst_ref=part_of(there(t).at[shard], t, at),
+            send_sem=ring_send.at[way, i, FIRST_PART[t] + u], recv_sem=ring_recv.at[shard, 2 * FIRST_PART[t] + at],
             device_id=dev, device_id_type=MESH,
         ))
 
     def arrived(t, i, at):
-        here = quarter(slot(t, i), at)
+        here = part_of(slot(t, i), t, at)
         pltpu.make_async_remote_copy(
-            src_ref=here, dst_ref=here, send_sem=ring_send.at[0, t, i, 0], recv_sem=ring_recv.at[t, order[i], at],
+            src_ref=here, dst_ref=here, send_sem=ring_send.at[0, i, 0], recv_sem=ring_recv.at[order[i], 2 * FIRST_PART[t] + at],
             device_id={"rep": 1 - rep}, device_id_type=MESH,
         ).wait_recv()
 
@@ -277,39 +282,58 @@
         ).wait_recv()
 
     def send_own(t):
-        for u in range(2):
+        for u in range(PARTS[t]):
             send(t, 0, u, UP)
             send(t, 0, u, BACK)
 
     def relay(t, i):
-        for u in range(2):
-            arrived(t, i, rep * 2 + u)
+        for u in range(PARTS[t]):
+            arrived(t, i, rep * PARTS[t] + u)
             send(t, i, u, UP)
             send(t, i, u, BACK)
             send(t, i, u, REP)
 
     def rest(t, i):
-        for u in range(2):
-            arrived(t, i, (1 - rep) * 2 + u)
+        for u in range(PARTS[t]):
+            arrived(t, i, (1 - rep) * PARTS[t] + u)
 
     loads[0].wait()
     loads[1].wait()
     wi_in[...] = wide_in[...].astype(bf16)
     wo_in[...] = wide_out[...].astype(bf16)
-    loads[2].wait()
-    loads[3].wait()
-
-    @pl.loop(0, slab // 32)
-    def _(j):
-        rows = pl.ds(pl.multiple_of(j * 32, 32), 32)
-        gu_in[rows, 0:units] = wide_gate[rows, :].astype(bf16)
-        gu_in[rows, units:] = wide_up[rows, :].astype(bf16)
+    def cast_gate_up(start, count):
+        @pl.loop(0, count // 32)
+        def _(j):
+            rows = pl.ds(pl.multiple_of(start + j * 32, 32), 32)
+            gu_in[rows, 0:units] = wide_gate[rows, :].astype(bf16)
+            gu_in[rows, units:] = wide_up[rows, :].astype(bf16)
 
     pl.semaphore_wait(barrier, n - 1 + 4)
     send_own(WI)
     send_own(WO)
-    send_own(GU)
+    loads[2].wait()
+    loads[3].wait()
+    for u in range(PARTS[GU]):
+        cast_gate_up(rep * half + u * (half // PARTS[GU]), half // PARTS[GU])
+        send(GU, 0, u, UP)
+        send(GU, 0, u, BACK)
+
+    def share_mixer(i):
+        for t, held, own in ((0, wi_all, wi_in), (1, wo_all, wo_in)):
+            src = own if i == 0 else held.at[0, order[i]]
+            remote(src, held.at[2, order[i]], tp_send.at[t, i, 1], tp_recv.at[t, i, 1], {"tp": across})
+            remote(src, held.at[1, order[i]], tp_send.at[t, i, 0], tp_recv.at[t, i, 0], {"tp": mate})
+
+    def pass_mixer(i):
+        for t, held in ((0, wi_all), (1, wo_all)):
+            landed(held.at[2, order[i]], tp_send.at[t, i, 1], tp_recv.at[t, i, 1])
+            remote(held.at[2, order[i]], held.at[3, order[i]], tp_send.at[t, i, 2], tp_recv.at[t, i, 2], {"tp": mate})
+
+    share_mixer(0)
     loads[4].wait()
+    loads[5].wait()
+    cast_gate_up((1 - rep) * half, half)
+    loads[6].wait()
 
     @pl.loop(0, units // 32)
     def _(j):
@@ -319,7 +343,7 @@
     for offset in range(1, n):
         remote(sc_in, sc_all.at[fs], sc_send.at[offset - 1], sc_recv.at[fs], to_fs(offset))
     for k in (1, 2, 3):
-        remote(ps_in, ps_all.at[k - 1], tp_send.at[2, k - 1], tp_recv.at[2, k - 1], {"tp": peers[k]})
+        remote(ps_in, ps_all.at[k - 1], tp_send.at[2, 0, k - 1], tp_recv.at[2, 0, k - 1], {"tp": peers[k]})
     own_wi = pltpu.make_async_copy(wi_in, wi_all.at[0, fs], loc.at[0])
     own_wo = pltpu.make_async_copy(wo_in, wo_all.at[0, fs], loc.at[1])
     own_wi.start()
@@ -371,20 +395,25 @@
     send_own(DN)
     for t in (WI, WO, GU):
         relay(t, 2)
+    rest(WI, 1)
+    rest(WO, 1)
+    share_mixer(1)
     rest(GU, 1)
     gate_up(1, False)
     for t in (WI, WO, GU):
         relay(t, 3)
+    pass_mixer(0)
+    rest(WI, 2)
+    rest(WO, 2)
+    share_mixer(2)
     rest(GU, 2)
     gate_up(2, False)
-    for t in (WI, WO):
-        for i in range(1, n):
-            rest(t, i)
+    rest(WI, 3)
+    rest(WO, 3)
+    share_mixer(3)
     own_wi.wait()
     own_wo.wait()
-    for k in (1, 2, 3):
-        remote(wi_all.at[0], wi_all.at[k], tp_send.at[0, k - 1], tp_recv.at[0, k - 1], {"tp": peers[k]})
-        remote(wo_all.at[0], wo_all.at[k], tp_send.at[1, k - 1], tp_recv.at[1, k - 1], {"tp": peers[k]})
+    pass_mixer(1)
     relay(DN, 1)
     rest(GU, 3)
     gate_up(3, False)
@@ -423,20 +452,24 @@
 
     scatter_one(0)
     relay(DN, 2)
+    pass_mixer(2)
     rest(DN, 1)
     scatter_one(1)
     gather_one(0)
     relay(DN, 3)
+    pass_mixer(3)
     rest(DN, 2)
     scatter_one(2)
     gather_one(1)
     rest(DN, 3)
     scatter_one(3)
     gather_one(2)
-    for t in (0, 1, 2):
-        for k in (1, 2, 3):
-            where = (wi_all.at[k], wo_all.at[k], ps_all.at[k - 1])[t]
-            landed(where, tp_send.at[t, k - 1], tp_recv.at[t, k - 1])
+    for k in (1, 2, 3):
+        landed(ps_all.at[k - 1], tp_send.at[2, 0, k - 1], tp_recv.at[2, 0, k - 1])
+    for i in range(n):
+        for t, held in ((0, wi_all), (1, wo_all)):
+            landed(held.at[1, order[i]], tp_send.at[t, i, 0], tp_recv.at[t, i, 0])
+            landed(held.at[3, order[i]], tp_send.at[t, i, 2], tp_recv.at[t, i, 2])
     gather_one(3)
 
     second[...] = normed_rows(r1[...], gains[1:2, :])
@@ -579,12 +612,12 @@
             pltpu.VMEM((n, 2, share, slab), bf16),
             pltpu.VMEM((n, share, slab), bf16),
             pltpu.VMEM((n, share, slab), bf16),
-            dma((3, 4, n, 2)), dma((4, n, QUARTERS)),
+            dma((3, n, FIRST_PART[-1])), dma((n, 2 * FIRST_PART[-1])),
             dma((n - 1,)), dma((n,)),
-            dma((3, 3)), dma((3, 3)),
+            dma((3, n, 3)), dma((3, n, 3)),
             dma((2 * n, 3)), dma((2 * n, 3)),
             dma((n + 1, 3)), dma((n + 1, 3)),
-            dma((7,)),
+            dma((9,)),
         ],
         compiler_params=pltpu.CompilerParams(
             collective_id=0, has_side_effects=True, vmem_limit_bytes=60 * 1024 * 1024

time: 179 us -> 151 us (0.84)
  Pallas kernels: 176 us -> 149 us
    pallas_call x1, Pallas kernels: 176 us -> 149 us  [fused_layer(): pl.pallas_call(functools.partial(layer_kernel, n), out_shape=jax.ShapeDty...]
where the time goes in v3:
time: 151 us
  Pallas kernels  149 us (99%)
  local copies, waits for them, and re-layouts  2.3 us (2%)
    pallas_call x1, Pallas kernels, fused_layer(): pl.pallas_call(functools.partial(layer_kernel, n), out_shape=jax.ShapeDty...  149 us

profile of v3, /device:TPU:0, one launch (start us, length us, event | category | flops | bytes accessed | tf_op | source)
XLA Modules:
  0.0 150.9 jit_solution(6847956184937494918)
XLA Ops:
  0.0 148.6 %shard_map.127 = bf16[256,2048]{1,0:T(8,128)(2,1)} custom-call(bf16[256,2048]{1,0:T(8,128)(2,1)} %tok.1, f32[3,2048]{1,0:T(4,128)} %gains.1, f32[512,768]{1,0:T(8,128)} %gate_hbm.1, f32[512,768]{1,0:T(8,128)} %up_hbm.1, f32[2,768]{1,0:T(2,128)} %hs.1, f32[768,512]{1,0:T(8,128)} %down_hbm.1, f32[512,512]{1,0:T(8,128)} %mix_in_hbm.1, f32[128,512]{1,0:T(8,128)} %mix_out_hbm.1, ...), custom_call_target="tpu_custom_call" | custom-call | tf_op jit(solution)/shard_map/pallas_call | solution.py:579
  148.6 2.3 %copy.15 = bf16[256,2048]{1,0:T(8,128)(2,1)} copy(bf16[256,2048]{1,0:T(8,128)(2,1)} %shard_map.127) | data formatting | bytes 2097152
